TPU v7x, 256 devices: a whole 4x4x8 slice. The times are simulated.
256 devices in a mesh: kv: 32 (over z, x), tp: 8 (over y, core).
Axes of the slice: x: 4, y: 4, z: 8, core: 2. Of those that a mesh axis runs over, the one named last changes fastest.
Arguments:
- inputs: bfloat16 [4, 8192, 2048], P(None, 'kv'), may hold values from -40 to 40
- query_weight: bfloat16 [2048, 2048], P(None, 'tp'), may hold values from -0.125 to 0.125
- key_weight: bfloat16 [2048, 1024], P(None, 'tp'), may hold values from -0.125 to 0.125
- value_weight: bfloat16 [2048, 1024], P(None, 'tp'), may hold values from -0.125 to 0.125
- out_weight: bfloat16 [2048, 2048], P('tp'), may hold values from -1 to 1
- chosen: int32 [4, 128, 32], P(None, 'kv'), may hold values from 0 to 127, as said below
- lengths: int32 [4], replicated, may hold values from 1 to 8192, 12288 in all
Outputs:
- mixed: bfloat16 [4, 8192, 2048], P(None, 'kv', 'tp')
Inputs may be any that keep to these rules, and one draw needn't show every extreme that they name: chosen[b, q, 0] = q; every entry names a block of the same sequence at or before q; entries may repeat. Over the query blocks of positions k * 256 to (k+1) * 256 - 1 of all sequences, the named blocks that lie in another span of 256 positions number at most 3 distinct blocks for each other span, and 3 is reached.
All inputs are finite; a program needn't handle non-finite values.
Results may differ from a plain program's by a relative error of at most 0.014.
The roundings to bfloat16 on the way count: a program that leaves them out, or rounds other values in their place, can miss the bound.
Values may be sent and summed in bfloat16 or wider, within the bound.
A program may use at most 128 MiB of HBM per device.

v0:
```python
import jax
import jax.numpy as jnp
from jax import lax
from jax.experimental import pallas as pl
from jax.experimental.pallas import tpu as pltpu
from jax.sharding import PartitionSpec as P

HD = 128
KB = 64
TOPK = 32
SEQS = 4
SPAN = 256
MODEL = 2048
NZ, NX, NY = 8, 4, 4
NTP = 8
REACH = (7, 5, 3, 2)
NEAR_REACH = (7, 2, 1, 0)
LANES = 128
MORE = 8
COUNT = 124
REPEATS, LOCAL, LIVE, ORDER = 0, 1, 2, 3
CHUNK = 256
MESH = pl.DeviceIdType.MESH
ANY = pl.BlockSpec(memory_space=pl.ANY)
SMEM = pl.BlockSpec(memory_space=pltpu.SMEM)
VMEM = pl.BlockSpec(memory_space=pltpu.VMEM)


def sequence_of(slot, lengths):
    size = [lengths[b] for b in range(SEQS)]
    found = jnp.int32(0)
    for b in range(SEQS):
        rank = jnp.int32(0)
        for o in range(SEQS):
            if o < b:
                rank += (size[o] >= size[b]).astype(jnp.int32)
            elif o > b:
                rank += (size[o] > size[b]).astype(jnp.int32)
        found += jnp.where(rank == slot, b, 0)
    return found


def project_kernel(lengths, x, key_w, value_w, chosen, kv_out, plan, weights, named, packed):
    @pl.when(pl.program_id(0) == 0)
    def _():
        weights[:, :HD] = key_w[...]
        weights[:, HD:] = value_w[...]

    kv_out[0] = jnp.dot(x[0], weights[...], preferred_element_type=jnp.float32).astype(jnp.bfloat16)

    @pl.when(pl.program_id(0) == 0)
    def _():
        kv = lax.axis_index("kv")
        named[...] = jnp.full(named.shape, -1, jnp.int32)
        for b in range(SEQS):
            named[b * 4:(b + 1) * 4, :TOPK] = chosen[b]
        block = named[...]
        lane = lax.broadcasted_iota(jnp.int32, block.shape, 1)
        row = lax.broadcasted_iota(jnp.int32, block.shape, 0)
        i = row % 4
        length = jnp.full(block.shape, lengths[0])
        for b in range(1, SEQS):
            length = jnp.where(row // 4 == b, lengths[b], length)
        member = jnp.zeros(block.shape, jnp.int32)
        for e in range(TOPK):
            member |= (block[:, e:e + 1] == lane).astype(jnp.int32)
        member = jnp.where((kv * 4 + i) * KB < length, member, 0)
        repeats = jnp.sum((block == kv * 4 + i).astype(jnp.int32), axis=1, keepdims=True) - 1
        here = lane - kv * 4
        inside = (here >= 0) & (here < 4)
        local = jnp.sum(jnp.where(inside, member << jnp.where(inside, here, 0), 0), axis=1, keepdims=True)
        named[...] = jnp.where(here < 0, member << i, 0)
        live = jnp.int32(0)
        for b in range(SEQS):
            live += (lengths[b] > kv * SPAN).astype(jnp.int32)
        more = jnp.where(lane == REPEATS, repeats, jnp.where(lane == LOCAL, local, live))
        for j in range(SEQS):
            more = jnp.where(lane == ORDER + j, sequence_of(j, lengths), more)
        plan[MORE:, :] = more

        packed[...] = jnp.zeros(packed.shape, jnp.int32)
        for b in range(SEQS):
            packed[b:b + 1, :] = jnp.sum(named[b * 4:(b + 1) * 4, :], axis=0, keepdims=True)
        code = packed[...]
        lane = lax.broadcasted_iota(jnp.int32, code.shape, 1)
        held = (code != 0).astype(jnp.int32)
        code = lane + 256 * code
        steps = (1, 2, 4, 8, 16, 32, 64)
        upto = held
        for s in steps:
            upto += jnp.where(lane >= s, pltpu.roll(upto, s, 1), 0)
        count = jnp.sum(held, axis=1, keepdims=True)
        gap = lane - (upto - 1)
        for s in steps:
            there = pltpu.roll(code, LANES - s, 1)
            there_gap = pltpu.roll(gap, LANES - s, 1)
            take = (pltpu.roll(held, LANES - s, 1) != 0) & ((there_gap & s) != 0)
            stay = (held != 0) & ((gap & s) == 0)
            code = jnp.where(take, there, code)
            gap = jnp.where(take, there_gap, gap)
            held = (take | stay).astype(jnp.int32)
        plan[:MORE, :] = jnp.where(lane == COUNT, count, code)


def project(lengths, inputs, key_weight, value_weight, chosen):
    once = dict(pipeline_mode=pl.Buffered(1))
    rows = MORE + SEQS * (SPAN // KB)
    return pl.pallas_call(
        project_kernel,
        name="project",
        out_shape=(
            jax.ShapeDtypeStruct((SEQS, SPAN, 2 * HD), jnp.bfloat16),
            jax.ShapeDtypeStruct((rows, LANES), jnp.int32),
        ),
        grid_spec=pltpu.PrefetchScalarGridSpec(
            num_scalar_prefetch=1,
            grid=(SEQS,),
            in_specs=[
                pl.BlockSpec((1, SPAN, MODEL), lambda j, lens: (sequence_of(j, lens), 0, 0)),
                pl.BlockSpec((MODEL, HD), lambda j, lens: (0, 0), **once),
                pl.BlockSpec((MODEL, HD), lambda j, lens: (0, 0), **once),
                pl.BlockSpec((SEQS, SPAN // KB, TOPK), lambda j, lens: (0, 0, 0), **once),
            ],
            out_specs=(
                pl.BlockSpec((1, SPAN, 2 * HD), lambda j, lens: (j, 0, 0)),
                pl.BlockSpec((rows, LANES), lambda j, lens: (0, 0)),
            ),
            scratch_shapes=[
                pltpu.VMEM((MODEL, 2 * HD), jnp.bfloat16),
                pltpu.VMEM((rows - MORE, LANES), jnp.int32),
                pltpu.VMEM((MORE, LANES), jnp.int32),
            ],
        ),
    )(lengths, inputs, key_weight, value_weight, chosen)


def spread_kernel(reach, own, out_w, inputs, query_w, cache, columns, q_out, rows_in, weights,
                  load_sem, recv, up_sem, top_sem, relay_up, relay_down, right_sem, left_sem, pass_right, pass_left, w_send, w_recv):
    kv, tp = lax.axis_index("kv"), lax.axis_index("tp")
    z, x = kv // NX, kv % NX
    right = {"kv": z * NX + (x + 1) % NX}
    left = {"kv": z * NX + (x + NX - 1) % NX}
    x_right, x_left, x_far = (x + 1) % NX, (x + NX - 1) % NX, (x + 2) % NX
    half = SPAN // 2

    def load_rows(b):
        return pltpu.make_async_copy(inputs.at[b], rows_in.at[b], load_sem.at[b])

    load_w = pltpu.make_async_copy(query_w, weights, load_sem.at[SEQS])
    load_w.start()
    for b in range(SEQS):
        load_rows(b).start()

    above = {"kv": (z + 1) % NZ * NX + x}
    below = {"kv": (z + NZ - 1) % NZ * NX + x}
    top = {"kv": (NZ - 1) * NX + x}

    barrier = pltpu.get_barrier_semaphore()

    def greet(device):
        pl.semaphore_signal(barrier, inc=1, device_id=device, device_id_type=MESH)

    for d in (above, below, right, left):
        greet(d)
    for d in range(1, NTP):
        greet({"tp": (tp + d) % NTP})
    low = (z >= 1) & (z <= 2)

    @pl.when(low)
    def _():
        greet(top)

    @pl.when(z == NZ - 1)
    def _():
        for w in (1, 2):
            greet({"kv": w * NX + x})

    pl.semaphore_wait(barrier, 4 + NTP - 1 + low.astype(jnp.int32) + z // (NZ - 1) * 2)

    def piece(slot, owner_z, owner_x, h):
        first = pl.multiple_of((owner_z * NX + owner_x) * SPAN + h * half, half)
        return cache.at[slot, pl.ds(first, half)]

    def mine(slot, h):
        return own.at[slot, pl.ds(h * half, half)]

    def send(src, sem, slot, owner_z, owner_x, h, device):
        return pltpu.make_async_remote_copy(
            src_ref=src, dst_ref=piece(slot, owner_z, owner_x, h), send_sem=sem,
            recv_sem=recv.at[slot, owner_z * NX + owner_x, h],
            device_id=device, device_id_type=MESH)

    def arrived(slot, owner_z, owner_x, h):
        here = piece(slot, owner_z, owner_x, h)
        send(here, up_sem.at[slot, 0, h], slot, owner_z, owner_x, h, right).wait_recv()

    def start(copy):
        copy.start()

    def wait_send(copy):
        copy.wait_send()

    def goes_up(slot, d):
        climb = 3 if slot == 0 else NZ
        return (z + 1 <= reach[slot]) & (d <= climb)

    columns_of = (x, x_left, x_far, x_right)

    def whole(d):
        return (d == z) & ((z <= 2) | (z >= 5))

    def relay(c, h, src, act):
        @pl.when(z < (3 if c == 0 else 2))
        def _():
            act(send(src, relay_up.at[c, h], 0, 0, columns_of[c], h, above))

        @pl.when((z == 0) | (z >= 6))
        def _():
            act(send(src, relay_down.at[c, h], 0, 0, columns_of[c], h, below))

    def relay_piece(c, h, act):
        relay(c, h, piece(0, 0, columns_of[c], h), act)

    def along(slot, t, d, h, src, act):
        w = z - d
        plain = jnp.logical_not(whole(d)) if slot == 0 else z >= 0
        beside = plain | (z == 0)

        @pl.when(plain & goes_up(slot, d))
        def _():
            act(send(src, up_sem.at[slot, t, h], slot, w, x, h, above))

        if slot == 0:
            @pl.when(plain & (d >= 6))
            def _():
                act(send(src, up_sem.at[slot, t, h], slot, w, x, h, below))

            @pl.when(whole(d))
            def _():
                relay(0, h, src, act)

        @pl.when(beside)
        def _():
            act(send(src, right_sem.at[slot, t, h], slot, w, x, h, right))
            act(send(src, left_sem.at[slot, t, h], slot, w, x, h, left))

    def to_top(h):
        return send(mine(0, h), top_sem.at[h], 0, z, x, h, top)

    def each(body, slots=range(SEQS)):
        for slot in slots:
            @pl.when(z <= reach[slot])
            def _(slot=slot):
                body(slot)

    def distance(t):
        return t % 2 * ((t + 1) // 2) + (1 - t % 2) * ((NZ - t // 2) % NZ)

    def passing(slot, t, w, act):
        act(send(piece(slot, w, x_left, 0), pass_right.at[slot, t], slot, w, x_left, 0, right))
        act(send(piece(slot, w, x_right, 1), pass_left.at[slot, t], slot, w, x_right, 1, left))

    def around(t, slots=range(SEQS)):
        d = distance(t)
        w = z - d

        def body(slot):
            arrived(slot, w, x_left, 0)
            arrived(slot, w, x_right, 1)
            if slot == 0:
                @pl.when(jnp.logical_not(whole(d)) | (z == 0))
                def _():
                    passing(slot, t, w, start)

                @pl.when(whole(d))
                def _():
                    relay_piece(1, 0, start)
                    relay_piece(3, 1, start)
            else:
                passing(slot, t, w, start)

        each(body, slots)

    late = ((1, 1), (3, 0), (2, 0), (2, 1))

    def tail(t):
        @pl.when(whole(distance(t)) & (z <= reach[0]))
        def _():
            for c, h in late:
                arrived(0, 0, columns_of[c], h)
                relay_piece(c, h, start)

    def column(t):
        d = distance(t)

        def body(slot):
            for h in range(2):
                arrived(slot, z - d, x, h)
                along(slot, t, d, h, piece(slot, z - d, x, h), start)

        each(body)

    def finish(t):
        d = distance(t)
        w = z - d

        def rest(slot):
            for c, h in late:
                arrived(slot, w, columns_of[c], h)

        def body(slot):
            for h in range(2):
                along(slot, t, d, h, piece(slot, w, x, h), wait_send)
            if slot == 0:
                @pl.when(jnp.logical_not(whole(d)))
                def _():
                    rest(slot)

                @pl.when(jnp.logical_not(whole(d)) | (z == 0))
                def _():
                    passing(slot, t, w, wait_send)

                @pl.when(whole(d))
                def _():
                    for c, h in ((1, 0), (3, 1)) + late:
                        relay_piece(c, h, wait_send)
            else:
                rest(slot)
                passing(slot, t, w, wait_send)

        each(body)

    def column_copy(d):
        peer = (tp + d) % NTP
        first = pl.multiple_of(peer * SPAN, SPAN)
        return pltpu.make_async_remote_copy(
            src_ref=out_w.at[:, pl.ds(first, SPAN)], dst_ref=columns.at[tp],
            send_sem=w_send.at[d - 1], recv_sem=w_recv.at[d - 1],
            device_id={"tp": peer}, device_id_type=MESH)

    def begin(slot):
        for h in range(2):
            along(slot, 0, 0, h, mine(slot, h), start)

    @pl.when(low)
    def _():
        for h in range(2):
            to_top(h).start()

    each(begin, (0, 1))

    load_w.wait()
    for b in range(SEQS):
        load_rows(b).wait()
        q_out[b] = jnp.dot(rows_in[b], weights[...], preferred_element_type=jnp.float32).astype(jnp.bfloat16)

    around(0, (0,))
    each(begin, (2, 3))
    for d in range(1, NTP):
        column_copy(d).start()

    @pl.loop(1, NZ + 2)
    def _(t):
        @pl.when((t < NZ) & (distance(t) <= z))
        def _():
            column(t)

        @pl.when((t <= NZ) & (t > 1) & (distance(t - 1) <= z))
        def _():
            around(t - 1)

        @pl.when(t == 1)
        def _():
            around(0, (1, 2, 3))

        @pl.when(t >= 2)
        def _():
            tail(t - 2)

    @pl.loop(0, NZ)
    def _(t):
        @pl.when(distance(t) <= z)
        def _():
            finish(t)

    @pl.when(low)
    def _():
        for h in range(2):
            to_top(h).wait_send()

    for d in range(1, NTP):
        column_copy(d).wait()


def spread(reach, own, out_weight, inputs, query_weight):
    dma = pltpu.SemaphoreType.DMA
    return pl.pallas_call(
        lambda *refs: spread_kernel(reach, *refs),
        name="spread",
        out_shape=(
            jax.ShapeDtypeStruct((SEQS, NZ * NX * SPAN, 2 * HD), jnp.bfloat16),
            jax.ShapeDtypeStruct((NTP, SPAN, SPAN), jnp.bfloat16),
            jax.ShapeDtypeStruct((SEQS, SPAN, 2 * HD), jnp.bfloat16),
        ),
        in_specs=[ANY] * 4,
        out_specs=(ANY, ANY, VMEM),
        scratch_shapes=[
            pltpu.VMEM((SEQS, SPAN, MODEL), jnp.bfloat16),
            pltpu.VMEM((MODEL, 2 * HD), jnp.bfloat16),
            dma((SEQS + 1,)),
            dma((SEQS, NZ * NX, 2)),
            dma((SEQS, NZ, 2)),
            dma((2,)),
            dma((NX, 2)),
            dma((NX, 2)),
            dma((SEQS, NZ, 2)),
            dma((SEQS, NZ, 2)),
            dma((SEQS, NZ)),
            dma((SEQS, NZ)),
            dma((NTP - 1,)),
            dma((NTP - 1,)),
        ],
        compiler_params=pltpu.CompilerParams(
            collective_id=0 if reach == REACH else 1, has_side_effects=True
        ),
    )(own, out_weight, inputs, query_weight)


def attend_kernel(lengths, plan, q, own, cache, out, keys, scores, high, total, acc, own_sems, sems):
    kv = lax.axis_index("kv")
    slots = plan[MORE, LIVE]
    blocks = SPAN // KB
    heads = 2

    def sequence(slot):
        b = plan[MORE, ORDER + slot]
        return b, plan[b, COUNT]

    def own_copy(slot):
        return pltpu.make_async_copy(own.at[slot], keys.at[slot % 2, pl.ds(0, SPAN)], own_sems.at[slot % 2])

    def block_copy(slot, block, e):
        row = pl.multiple_of(block * KB, KB)
        to = pl.multiple_of(SPAN + e * KB, KB)
        return pltpu.make_async_copy(
            cache.at[slot, pl.ds(row, KB)], keys.at[slot % 2, pl.ds(to, KB)], sems.at[slot % 2])

    def fetch(slot):
        b, n = sequence(slot)
        own_copy(slot).start()

        @pl.loop(0, n)
        def _(e):
            block_copy(slot, plan[b, e] % 256, e).start()

        past = pl.ds(pl.multiple_of(SPAN + n * KB, KB), 3 * KB)
        keys[slot % 2, past, :] = jnp.zeros((3 * KB, 2 * HD), jnp.bfloat16)

    def part(h, i):
        return slice(h * SPAN + i * KB, h * SPAN + (i + 1) * KB)

    def compute(slot):
        b, n = sequence(slot)
        held = keys.at[slot % 2]
        chunks = 1 + (n + 3) // 4
        own_copy(slot).wait()
        both = q[b]
        stacked = jnp.concatenate([both[:, :HD], both[:, HD:]], axis=0)
        lane = lax.broadcasted_iota(jnp.int32, (1, CHUNK), 1)
        place = lane // KB

        def score(first):
            return lax.dot_general(stacked, held[pl.ds(first, CHUNK), :HD], (((1,), (1,)), ((), ())),
                                   preferred_element_type=jnp.float32) * (HD ** -0.5)

        s = score(0)
        col = lax.broadcasted_iota(jnp.int32, (KB, CHUNK), 1)
        row = lax.broadcasted_iota(jnp.int32, (KB, CHUNK), 0)
        for i in range(blocks):
            bits = plan[MORE + b * 4 + i, LOCAL] | (1 << i)
            named = jnp.zeros((1, CHUNK), jnp.int32)
            for p in range(blocks):
                named = jnp.where(place == p, (bits >> p) & 1, named)
            limit = jnp.where(named != 0, lane, SPAN)
            for h in range(heads):
                now = jnp.where(limit <= row + i * KB, s[part(h, i)], -jnp.inf)
                scores[0, part(h, i), :] = now
                high[part(h, i), :] = jnp.maximum(now[:, :HD], now[:, HD:])

        @pl.loop(0, n)
        def _(e):
            block_copy(slot, 0, e).wait()

        @pl.loop(1, chunks)
        def _(c):
            s = score(pl.multiple_of(c * CHUNK, CHUNK))
            codes = []
            for p in range(blocks):
                e = (c - 1) * 4 + p
                codes.append(jnp.where(e < n, plan[b, e] // 256, 0))
            for i in range(blocks):
                shift = jnp.zeros((1, CHUNK), jnp.float32)
                for p in range(blocks):
                    absent = jnp.where((codes[p] >> i) & 1 != 0, jnp.float32(0), -jnp.inf)
                    shift = jnp.where(place == p, absent, shift)
                for h in range(heads):
                    now = s[part(h, i)] + shift
                    scores[c, part(h, i), :] = now
                    high[part(h, i), :] = jnp.maximum(high[part(h, i), :], jnp.maximum(now[:, :HD], now[:, HD:]))

        for h in range(heads):
            for i in range(blocks):
                top = jnp.max(high[part(h, i), :], axis=1, keepdims=True)
                high[part(h, i), :] = jnp.broadcast_to(top, (KB, HD))
        total[...] = jnp.zeros_like(total)

        @pl.loop(0, chunks)
        def _(c):
            for h in range(heads):
                for i in range(blocks):
                    top = high[part(h, i), :]
                    left = jnp.exp(scores[c, part(h, i), :HD] - top)
                    right = jnp.exp(scores[c, part(h, i), HD:] - top)
                    scores[c, part(h, i), :HD] = left
                    scores[c, part(h, i), HD:] = right
                    total[part(h, i), :] += left + right

        again = jnp.int32(0)
        for i in range(blocks):
            again += plan[MORE + b * 4 + i, REPEATS]

        def self_part(h, i):
            return jnp.where(col == row + i * KB, scores[0, part(h, i), :], 0.0)

        @pl.when(again > 0)
        def _():
            for h in range(heads):
                for i in range(blocks):
                    e = self_part(h, i)
                    times = plan[MORE + b * 4 + i, REPEATS].astype(jnp.float32)
                    total[part(h, i), :] += times * (e[:, :HD] + e[:, HD:])

        for h in range(heads):
            for i in range(blocks):
                share = 1.0 / jnp.sum(total[part(h, i), :], axis=1, keepdims=True)
                total[part(h, i), :] = jnp.broadcast_to(share, (KB, HD))
        acc[...] = jnp.zeros_like(acc)

        @pl.when(again > 0)
        def _():
            for h in range(heads):
                for i in range(blocks):
                    share = total[part(h, i), :]
                    e = self_part(h, i)
                    weight = jnp.concatenate([e[:, :HD] * share, e[:, HD:] * share], axis=1)
                    times = plan[MORE + b * 4 + i, REPEATS].astype(jnp.float32)
                    acc[part(h, i), :] = times * jnp.dot(
                        weight.astype(jnp.bfloat16), held[:SPAN, HD:], preferred_element_type=jnp.float32)

        @pl.loop(0, chunks)
        def _(c):
            share = total[...]
            weight = jnp.concatenate([scores[c, :, :HD] * share, scores[c, :, HD:] * share], axis=1)
            acc[...] += jnp.dot(weight.astype(jnp.bfloat16),
                                held[pl.ds(pl.multiple_of(c * CHUNK, CHUNK), CHUNK), HD:],
                                preferred_element_type=jnp.float32)

        pos = kv * SPAN + lax.broadcasted_iota(jnp.int32, (SPAN, HD), 0)
        for h in range(heads):
            done = jnp.where(pos < lengths[b], acc[h * SPAN:(h + 1) * SPAN, :], 0.0)
            out[slot, :, h * HD:(h + 1) * HD] = done.astype(jnp.bfloat16)

    @pl.when(slots > 0)
    def _():
        fetch(jnp.int32(0))

    @pl.loop(0, slots)
    def _(slot):
        @pl.when(slot + 1 < slots)
        def _():
            fetch(slot + 1)

        compute(slot)


def attend(lengths, plan, q, own, cache):
    most = NZ * NX * (SPAN // KB)
    rows = 2 * SPAN
    return pl.pallas_call(
        attend_kernel,
        name="attend",
        out_shape=jax.ShapeDtypeStruct((SEQS, SPAN, 2 * HD), jnp.bfloat16),
        in_specs=[SMEM, SMEM, VMEM, ANY, ANY],
        out_specs=VMEM,
        scratch_shapes=[
            pltpu.VMEM((2, SPAN + most * KB, 2 * HD), jnp.bfloat16),
            pltpu.VMEM((1 + most // 4, rows, CHUNK), jnp.float32),
            pltpu.VMEM((rows, HD), jnp.float32),
            pltpu.VMEM((rows, HD), jnp.float32),
            pltpu.VMEM((rows, HD), jnp.float32),
            pltpu.SemaphoreType.DMA((2,)),
            pltpu.SemaphoreType.DMA((2,)),
        ],
    )(lengths, plan, q, own, cache)


def collect_kernel(reach, own, groups, next_recv, prev_recv, core_recv, next_send, prev_send,
                   next_pass, prev_pass, core_send):
    kv, tp = lax.axis_index("kv"), lax.axis_index("tp")
    z = kv // NX
    y, core = tp // 2, tp % 2
    y_next, y_prev, y_far = (y + 1) % NY, (y + NY - 1) % NY, (y + 2) % NY
    after, before = {"tp": y_next * 2 + core}, {"tp": y_prev * 2 + core}
    partner = {"tp": y * 2 + 1 - core}
    half = SPAN // 2

    barrier = pltpu.get_barrier_semaphore()
    for d in (after, before, partner):
        pl.semaphore_signal(barrier, inc=1, device_id=d, device_id_type=MESH)
    pl.semaphore_wait(barrier, 3)

    def piece(owner_y, owner_core, slot, h):
        return groups.at[owner_y * 2 + owner_core, slot, pl.ds(h * half, half)]

    def copy(src, dst, send_sem, recv_sem, device):
        return pltpu.make_async_remote_copy(
            src_ref=src, dst_ref=dst, send_sem=send_sem, recv_sem=recv_sem,
            device_id=device, device_id_type=MESH)

    def mine(slot, h):
        return own.at[slot, pl.ds(h * half, half)]

    def to_next(slot, h):
        return copy(mine(slot, h), piece(y, core, slot, h), next_send.at[slot, h],
                    next_recv.at[0, slot, h], after)

    def to_prev(slot, h):
        return copy(mine(slot, h), piece(y, core, slot, h), prev_send.at[slot, h],
                    prev_recv.at[0, slot, h], before)

    def on_next(slot):
        here = piece(y_prev, core, slot, 0)
        return copy(here, here, next_pass.at[slot], next_recv.at[1, slot, 0], after)

    def on_prev(slot):
        here = piece(y_next, core, slot, 1)
        return copy(here, here, prev_pass.at[slot], prev_recv.at[1, slot, 1], before)

    def across(far, owner_y, slot, h, src=None):
        here = piece(owner_y, core, slot, h)
        return copy(here if src is None else src, here, core_send.at[far, slot, h],
                    core_recv.at[far, slot, h], partner)

    def each(body):
        for slot in range(SEQS):
            @pl.when(z <= reach[slot])
            def _(slot=slot):
                body(slot)

    def begin(slot):
        to_next(slot, 0).start()
        to_prev(slot, 1).start()
        to_next(slot, 1).start()
        to_prev(slot, 0).start()
        for h in range(2):
            across(0, y, slot, h, mine(slot, h)).start()

    def relay(slot):
        to_next(slot, 0).wait_recv()
        on_next(slot).start()
        across(1, y_prev, slot, 0).start()
        to_prev(slot, 1).wait_recv()
        on_prev(slot).start()
        across(2, y_next, slot, 1).start()
        to_next(slot, 1).wait_recv()
        across(1, y_prev, slot, 1).start()
        to_prev(slot, 0).wait_recv()
        across(2, y_next, slot, 0).start()

    def far(slot):
        on_next(slot).wait_recv()
        across(3, y_far, slot, 0).start()
        on_prev(slot).wait_recv()
        across(3, y_far, slot, 1).start()

    def finish(slot):
        for h in range(2):
            to_next(slot, h).wait_send()
            to_prev(slot, h).wait_send()
            across(0, y, slot, h).wait()
            across(1, y_prev, slot, h).wait()
            across(2, y_next, slot, h).wait()
            across(3, y_far, slot, h).wait()
        on_next(slot).wait_send()
        on_prev(slot).wait_send()

    each(begin)
    each(relay)
    each(far)
    each(finish)


def collect(reach, own):
    dma = pltpu.SemaphoreType.DMA
    return pl.pallas_call(
        lambda *refs: collect_kernel(reach, *refs),
        name="collect",
        out_shape=jax.ShapeDtypeStruct((NTP, SEQS, SPAN, 2 * HD), jnp.bfloat16),
        in_specs=[ANY],
        out_specs=ANY,
        scratch_shapes=[
            dma((2, SEQS, 2)),
            dma((2, SEQS, 2)),
            dma((4, SEQS, 2)),
            dma((SEQS, 2)),
            dma((SEQS, 2)),
            dma((SEQS,)),
            dma((SEQS,)),
            dma((4, SEQS, 2)),
        ],
        compiler_params=pltpu.CompilerParams(collective_id=2 if reach == REACH else 3, has_side_effects=True),
    )(own)


def mix_kernel(plan, own, groups, out_w, columns, out):
    tp = lax.axis_index("tp")
    live = pl.program_id(0) < plan[MORE, LIVE]

    @pl.when(live)
    def _():
        total = jnp.zeros((SPAN, SPAN), jnp.float32)
        own_w = out_w[:, pl.ds(pl.multiple_of(tp * SPAN, SPAN), SPAN)]
        for g in range(NTP):
            rows = jnp.where(tp == g, own[0], groups[g, 0])
            cols = jnp.where(tp == g, own_w, columns[g])
            part = jnp.dot(rows, cols, preferred_element_type=jnp.float32)
            total += part.astype(jnp.bfloat16).astype(jnp.float32)
        out[0] = total.astype(jnp.bfloat16)

    @pl.when(jnp.logical_not(live))
    def _():
        out[0] = jnp.zeros((SPAN, SPAN), jnp.bfloat16)


def mix(plan, own, groups, out_weight, columns):
    once = dict(pipeline_mode=pl.Buffered(1))

    def slot(j, plan):
        return jnp.minimum(j, jnp.maximum(plan[MORE, LIVE] - 1, 0))

    return pl.pallas_call(
        mix_kernel,
        name="mix",
        out_shape=jax.ShapeDtypeStruct((SEQS, SPAN, SPAN), jnp.bfloat16),
        grid_spec=pltpu.PrefetchScalarGridSpec(
            num_scalar_prefetch=1,
            grid=(SEQS,),
            in_specs=[
                pl.BlockSpec((1, SPAN, 2 * HD), lambda j, plan: (slot(j, plan), 0, 0)),
                pl.BlockSpec((NTP, 1, SPAN, 2 * HD), lambda j, plan: (0, slot(j, plan), 0, 0)),
                pl.BlockSpec((SPAN, MODEL), lambda j, plan: (0, 0), **once),
                pl.BlockSpec((NTP, SPAN, SPAN), lambda j, plan: (0, 0, 0), **once),
            ],
            out_specs=pl.BlockSpec((1, SPAN, SPAN), lambda j, plan: (plan[MORE, ORDER + j], 0, 0)),
        ),
    )(plan, own, groups, out_weight, columns)


def shards(inputs, query_weight, key_weight, value_weight, out_weight, chosen, lengths):
    own, plan = project(lengths, inputs, key_weight, value_weight, chosen)

    def rest(reach):
        cache, columns, queries = spread(reach, own, out_weight, inputs, query_weight)
        attended = attend(lengths, plan, queries, own, cache)
        groups = collect(reach, attended)
        return mix(plan, attended, groups, out_weight, columns)

    near = jnp.bool_(True)
    for j in range(1, SEQS):
        longer = jnp.sum((lengths > (NEAR_REACH[j] + 1) * NX * SPAN).astype(jnp.int32))
        near &= longer <= j
    return lax.cond(near, lambda: rest(NEAR_REACH), lambda: rest(REACH))


def solution(mesh):
    placed = (
        P(None, "kv", None),
        P(None, "tp"),
        P(None, "tp"),
        P(None, "tp"),
        P("tp", None),
        P(None, "kv", None),
        P(),
    )
    return jax.shard_map(
        shards, mesh=mesh, in_specs=placed, out_specs=P(None, "kv", "tp"), check_vma=False
    )
```

profile of v0, /device:TPU:1, one launch (start us, length us, event | category | flops | bytes accessed | tf_op | source)
XLA Modules:
  0.0 81.3 jit_solution(1860276679356589458)
XLA Ops:
  0.0 0.0 copy-start.3
  0.0 0.0 copy-start
  0.0 0.0 copy-start.1
  0.0 1.5 %fusion.2 = (s32[]{:T(128)}, s32[]{:T(128)}, s32[]{:T(128)}) fusion(s32[4]{0:T(128)} %lengths.1), kind=kLoop, calls=%fused_computation.5 | loop fusion | flops 33 | bytes 28 | tf_op jit(solution)/shard_map/reduce_sum | solution.py:780
  3.4 6.3 %project.1 = (bf16[4,256,256]{2,1,0:T(8,128)(2,1)S(1)}, s32[24,128]{1,0:T(8,128)S(1)}) custom-call(s32[4]{0:T(128)} %lengths.1, bf16[4,256,2048]{2,1,0:T(8,128)(2,1)} %x.1, bf16[2048,128]{1,0:T(8,128)(2,1)} %key_w.1, bf16[2048,128]{1,0:T(8,128)(2,1)} %value_w.1, s32[4,4,32]{2,1,0:T(4,128)} %chosen.1), custom_call_target="tpu_custom_call" | custom-call | tf_op jit(solution)/shard_map/project/pallas_call | solution.py:108
  9.7 0.0 copy-done.3
  9.7 0.0 copy-done
  9.7 0.0 copy-done.1
  9.7 70.8 %conditional.1 = (bf16[4,256,256]{2,1,0:T(8,128)(2,1)S(1)}) conditional(s32[]{:T(128)} %convert_element_type.15, (bf16[4,256,256]{2,1,0:T(8,128)(2,1)S(1)}, bf16[256,2048]{1,0:T(8,128)(2,1)S(1)}, bf16[4,256,2048]{2,1,0:T(8,128)(2,1)}, bf16[2048,256]{1,0:T(8,128)(2,1)S(1)}, s32[4]{0:T(128)S(1)}, /*index=5*/s32[24,128]{1,0:T(8,128)S(1)}) %tuple.23, ...), branch_computations={%region_3.0_spmd, %region_4.0_spmd} | conditional | bytes 8 | solution.py:782
  9.7 31.9 %spread.3 = (bf16[4,8192,256]{2,1,0:T(8,128)(2,1)}, bf16[8,256,256]{2,1,0:T(8,128)(2,1)}, bf16[4,256,256]{2,1,0:T(8,128)(2,1)}) custom-call(bf16[4,256,256]{2,1,0:T(8,128)(2,1)S(1)} %get-tuple-element.43.refs_0_.own, bf16[256,2048]{1,0:T(8,128)(2,1)S(1)} %get-tuple-element.44.refs_1_.out_w, bf16[4,256,2048]{2,1,0:T(8,128)(2,1)} %get-tuple-element.45.refs_2_, ...), custom_call_target="tpu_custom_call" | custom-call | tf_op jit(solution)/shard_map/cond/branch_1_fun/spread/pallas_call | solution.py:397
  41.7 7.5 %attend.3.refs_0_.own = bf16[4,256,256]{2,1,0:T(8,128)(2,1)} custom-call(s32[4]{0:T(128)S(1)} %get-tuple-element.42.lengths, s32[24,128]{1,0:T(8,128)S(1)} %get-tuple-element.41.plan, bf16[4,256,256]{2,1,0:T(8,128)(2,1)} %get-tuple-element.47.q, bf16[4,256,256]{2,1,0:T(8,128)(2,1)S(1)} %get-tuple-element.43.refs_0_.own, ...), custom_call_target="tpu_custom_call" | custom-call | tf_op jit(solution)/shard_map/cond/branch_1_fun/attend/pallas_call | solution.py:589
  49.1 25.9 %collect.3.groups = bf16[8,4,256,256]{3,2,1,0:T(8,128)(2,1)} custom-call(bf16[4,256,256]{2,1,0:T(8,128)(2,1)} %attend.3.refs_0_.own), custom_call_target="tpu_custom_call" | custom-call | tf_op jit(solution)/shard_map/cond/branch_1_fun/collect/pallas_call | solution.py:705
  75.1 5.2 %mix.3 = bf16[4,256,256]{2,1,0:T(8,128)(2,1)S(1)} custom-call(s32[24,128]{1,0:T(8,128)S(1)} %get-tuple-element.41.plan, bf16[4,256,256]{2,1,0:T(8,128)(2,1)} %attend.3.refs_0_.own, bf16[8,4,256,256]{3,2,1,0:T(8,128)(2,1)} %collect.3.groups, bf16[256,2048]{1,0:T(8,128)(2,1)S(1)} %get-tuple-element.44.refs_1_.out_w, bf16[8,256,256]{2,1,0:T(8,128)(2,1)} %get-tuple-element.49.columns), custom_call_target="tpu_custom_call" | custom-call | tf_op jit(solution)/shard_map/cond/branch_1_fun/mix/pallas_call | solution.py:751
  80.5 0.0 copy-start.2
  80.6 0.8 copy-done.2
Async XLA Ops:
  0.0 9.7 %copy-start.3 = (s32[4]{0:T(128)S(1)}, s32[4]{0:T(128)}, u32[]{:S(2)}) copy-start(s32[4]{0:T(128)} %lengths.1) | copy-start | bytes 52
  0.0 9.7 %copy-start = (bf16[256,2048]{1,0:T(8,128)(2,1)S(1)}, bf16[256,2048]{1,0:T(8,128)(2,1)}, u32[]{:S(2)}) copy-start(bf16[256,2048]{1,0:T(8,128)(2,1)} %param.13) | copy-start | bytes 3145732
  0.0 9.7 %copy-start.1 = (bf16[2048,256]{1,0:T(8,128)(2,1)S(1)}, bf16[2048,256]{1,0:T(8,128)(2,1)}, u32[]{:S(2)}) copy-start(bf16[2048,256]{1,0:T(8,128)(2,1)} %param.10) | copy-start | bytes 3145732
  80.5 0.8 copy-start.2
where the time goes:
time: 81.8 us; the launch traced here: 81.3 us
  Pallas kernels  76.8 us (94%)
  between operations  1.95 us (2%)
  other arithmetic  1.51 us (2%)
    pallas_call x1, Pallas kernels, spread(): pl.pallas_call(lambda *refs: spread_kernel(reach, *refs), name='spread',...  31.9 us
    pallas_call x1, Pallas kernels, collect(): pl.pallas_call(lambda *refs: collect_kernel(reach, *refs), name='collect'...  25.9 us
    pallas_call x1, Pallas kernels, attend(): pl.pallas_call(attend_kernel, name='attend', out_shape=jax.ShapeDtypeStru...  7.46 us
    pallas_call x1, Pallas kernels, project(): pl.pallas_call(project_kernel, name='project', out_shape=(jax.ShapeDtypeS...  6.27 us
    pallas_call x1, Pallas kernels, mix(): pl.pallas_call(mix_kernel, name='mix', out_shape=jax.ShapeDtypeStruct((SE...  5.24 us

commit v1 on v0

v1 whole, which is shorter than its diff:
```python
import jax
import jax.numpy as jnp
from jax import lax
from jax.experimental import pallas as pl
from jax.experimental.pallas import tpu as pltpu
from jax.sharding import PartitionSpec as P

HD = 128
KB = 64
TOPK = 32
SEQS = 4
SPAN = 256
MODEL = 2048
NZ, NX, NY = 8, 4, 4
NTP = 8
REACH = (7, 5, 3, 2)
NEAR_REACH = (7, 2, 1, 0)
LANES = 128
MORE = 8
COUNT = 124
REPEATS, LOCAL, LIVE, ORDER = 0, 1, 2, 3
CHUNK = 256
MESH = pl.DeviceIdType.MESH
ANY = pl.BlockSpec(memory_space=pl.ANY)
SMEM = pl.BlockSpec(memory_space=pltpu.SMEM)
VMEM = pl.BlockSpec(memory_space=pltpu.VMEM)


def sequence_of(slot, lengths):
    size = [lengths[b] for b in range(SEQS)]
    found = jnp.int32(0)
    for b in range(SEQS):
        rank = jnp.int32(0)
        for o in range(SEQS):
            if o < b:
                rank += (size[o] >= size[b]).astype(jnp.int32)
            elif o > b:
                rank += (size[o] > size[b]).astype(jnp.int32)
        found += jnp.where(rank == slot, b, 0)
    return found


def make_plan(kv, lengths, chosen, plan, named, packed):
    named[...] = jnp.full(named.shape, -1, jnp.int32)
    for b in range(SEQS):
        named[b * 4:(b + 1) * 4, :TOPK] = chosen[b]
    block = named[...]
    lane = lax.broadcasted_iota(jnp.int32, block.shape, 1)
    row = lax.broadcasted_iota(jnp.int32, block.shape, 0)
    i = row % 4
    length = jnp.full(block.shape, lengths[0])
    for b in range(1, SEQS):
        length = jnp.where(row // 4 == b, lengths[b], length)
    member = jnp.zeros(block.shape, jnp.int32)
    for e in range(TOPK):
        member |= (block[:, e:e + 1] == lane).astype(jnp.int32)
    member = jnp.where((kv * 4 + i) * KB < length, member, 0)
    repeats = jnp.sum((block == kv * 4 + i).astype(jnp.int32), axis=1, keepdims=True) - 1
    here = lane - kv * 4
    inside = (here >= 0) & (here < 4)
    local = jnp.sum(jnp.where(inside, member << jnp.where(inside, here, 0), 0), axis=1, keepdims=True)
    named[...] = jnp.where(here < 0, member << i, 0)
    live = jnp.int32(0)
    for b in range(SEQS):
        live += (lengths[b] > kv * SPAN).astype(jnp.int32)
    more = jnp.where(lane == REPEATS, repeats, jnp.where(lane == LOCAL, local, live))
    for j in range(SEQS):
        more = jnp.where(lane == ORDER + j, sequence_of(j, lengths), more)
    plan[MORE:, :] = more

    packed[...] = jnp.zeros(packed.shape, jnp.int32)
    for b in range(SEQS):
        packed[b:b + 1, :] = jnp.sum(named[b * 4:(b + 1) * 4, :], axis=0, keepdims=True)
    code = packed[...]
    lane = lax.broadcasted_iota(jnp.int32, code.shape, 1)
    held = (code != 0).astype(jnp.int32)
    code = lane + 256 * code
    steps = (1, 2, 4, 8, 16, 32, 64)
    upto = held
    for s in steps:
        upto += jnp.where(lane >= s, pltpu.roll(upto, s, 1), 0)
    count = jnp.sum(held, axis=1, keepdims=True)
    gap = lane - (upto - 1)
    for s in steps:
        there = pltpu.roll(code, LANES - s, 1)
        there_gap = pltpu.roll(gap, LANES - s, 1)
        take = (pltpu.roll(held, LANES - s, 1) != 0) & ((there_gap & s) != 0)
        stay = (held != 0) & ((gap & s) == 0)
        code = jnp.where(take, there, code)
        gap = jnp.where(take, there_gap, gap)
        held = (take | stay).astype(jnp.int32)
    plan[:MORE, :] = jnp.where(lane == COUNT, count, code)


def spread_kernel(reach, lengths, chosen, inputs, query_w, key_w, value_w, out_w,
                  cache, columns, q_out, plan, held, rows_in, q_weights, kv_weights, projected,
                  named, packed, load_sem, store_sem, recv, up_sem, beside_sem, once_sem):
    kv, tp = lax.axis_index("kv"), lax.axis_index("tp")
    z, x = kv // NX, kv % NX
    right = {"kv": z * NX + (x + 1) % NX}
    left = {"kv": z * NX + (x + NX - 1) % NX}
    x_right, x_left, x_far = (x + 1) % NX, (x + NX - 1) % NX, (x + 2) % NX
    half = SPAN // 2
    TO_TOP, RELAY_UP, RELAY_DOWN, W_SEND, W_RECV = range(5)
    COLUMN, LEFT, RIGHT, LATE = 0, 2, 3, 4

    loads = [
        pltpu.make_async_copy(key_w, kv_weights.at[:, pl.ds(0, HD)], load_sem.at[0]),
        pltpu.make_async_copy(value_w, kv_weights.at[:, pl.ds(HD, HD)], load_sem.at[1]),
    ]
    loads += [pltpu.make_async_copy(inputs.at[b], rows_in.at[b], load_sem.at[2 + b]) for b in range(SEQS)]
    load_q = pltpu.make_async_copy(query_w, q_weights, load_sem.at[2 + SEQS])
    for load in loads:
        load.start()
    load_q.start()

    above = {"kv": (z + 1) % NZ * NX + x}
    below = {"kv": (z + NZ - 1) % NZ * NX + x}
    top = {"kv": (NZ - 1) * NX + x}

    barrier = pltpu.get_barrier_semaphore()

    def greet(device):
        pl.semaphore_signal(barrier, inc=1, device_id=device, device_id_type=MESH)

    for d in (above, below, right, left):
        greet(d)
    for d in range(1, NTP):
        greet({"tp": (tp + d) % NTP})
    low = (z >= 1) & (z <= 2)

    @pl.when(low)
    def _():
        greet(top)

    @pl.when(z == NZ - 1)
    def _():
        for w in (1, 2):
            greet({"kv": w * NX + x})

    loads[0].wait()
    loads[1].wait()
    for b in range(SEQS):
        loads[2 + b].wait()
        projected[b] = jnp.dot(rows_in[b], kv_weights[...], preferred_element_type=jnp.float32).astype(jnp.bfloat16)
    for slot in range(SEQS):
        held[slot, pl.ds(pl.multiple_of(kv * SPAN, SPAN), SPAN), :] = projected[sequence_of(slot, lengths)]

    pl.semaphore_wait(barrier, 4 + NTP - 1 + low.astype(jnp.int32) + z // (NZ - 1) * 2)

    def piece(slot, owner_z, owner_x, h):
        first = pl.multiple_of((owner_z * NX + owner_x) * SPAN + h * half, half)
        return held.at[slot, pl.ds(first, half)]

    def mine(slot, h):
        return piece(slot, z, x, h)

    def store(slot, w):
        span = pl.ds(pl.multiple_of(w * NX * SPAN, NX * SPAN), NX * SPAN)
        return pltpu.make_async_copy(held.at[slot, span], cache.at[slot, span], store_sem.at[row(slot, w)])

    def row(slot, w):
        return sum(reach[o] + 1 for o in range(slot)) + w

    def send(src, sem, slot, owner_z, owner_x, h, kind, device):
        return pltpu.make_async_remote_copy(
            src_ref=src, dst_ref=piece(slot, owner_z, owner_x, h), send_sem=sem,
            recv_sem=recv.at[row(slot, owner_z), kind],
            device_id=device, device_id_type=MESH)

    def arrived(slot, w, kind):
        size = SPAN * 2 if kind == LATE else half
        there = held.at[slot, pl.ds(0, size)]
        pltpu.make_async_remote_copy(
            src_ref=there, dst_ref=there, send_sem=up_sem.at[row(slot, w)],
            recv_sem=recv.at[row(slot, w), kind], device_id=right, device_id_type=MESH).wait_recv()

    def sent(slot, sem, pieces):
        there = held.at[slot, pl.ds(0, pieces * half)]
        pltpu.make_async_remote_copy(
            src_ref=there, dst_ref=there, send_sem=sem, recv_sem=recv.at[0, 0],
            device_id=right, device_id_type=MESH).wait_send()

    def goes_up(slot, d):
        climb = 3 if slot == 0 else NZ
        return (z + 1 <= reach[slot]) & (d <= climb)

    columns_of = (x, x_left, x_far, x_right)

    def whole(d):
        return (d == z) & ((z <= 2) | (z >= 5))

    def relay(c, h, kind):
        src = piece(0, 0, columns_of[c], h)

        @pl.when(z < (3 if c == 0 else 2))
        def _():
            send(src, once_sem.at[RELAY_UP], 0, 0, columns_of[c], h, kind, above).start()

        @pl.when((z == 0) | (z >= 6))
        def _():
            send(src, once_sem.at[RELAY_DOWN], 0, 0, columns_of[c], h, kind, below).start()

    def plain(slot, d):
        return jnp.logical_not(whole(d)) if slot == 0 else z >= 0

    def onward(slot, d):
        up = plain(slot, d) & goes_up(slot, d)
        down = plain(slot, d) & (d >= 6) if slot == 0 else z < 0
        return up, down

    def along(slot, d, h):
        w = z - d
        src = piece(slot, w, x, h)
        up, down = onward(slot, d)

        @pl.when(up)
        def _():
            send(src, up_sem.at[row(slot, w)], slot, w, x, h, COLUMN + h, above).start()

        if slot == 0:
            @pl.when(down)
            def _():
                send(src, up_sem.at[row(slot, w)], slot, w, x, h, COLUMN + h, below).start()

            @pl.when(whole(d))
            def _():
                relay(0, h, COLUMN + h)

        @pl.when(plain(slot, d) | (z == 0))
        def _():
            sem = beside_sem.at[row(slot, w)]
            send(src, sem, slot, w, x, h, LEFT if h == 0 else LATE, right).start()
            send(src, sem, slot, w, x, h, LATE if h == 0 else RIGHT, left).start()

    def to_top(h):
        return send(mine(0, h), once_sem.at[TO_TOP], 0, z, x, h, COLUMN + h, top)

    def each(body, slots=range(SEQS)):
        for slot in slots:
            @pl.when(z <= reach[slot])
            def _(slot=slot):
                body(slot)

    def distance(t):
        return t % 2 * ((t + 1) // 2) + (1 - t % 2) * ((NZ - t // 2) % NZ)

    def around(t, slots=range(SEQS)):
        d = distance(t)
        w = z - d

        def passing(slot):
            sem = beside_sem.at[row(slot, w)]
            send(piece(slot, w, x_left, 0), sem, slot, w, x_left, 0, LATE, right).start()
            send(piece(slot, w, x_right, 1), sem, slot, w, x_right, 1, LATE, left).start()

        def body(slot):
            arrived(slot, w, LEFT)
            arrived(slot, w, RIGHT)
            if slot == 0:
                @pl.when(plain(slot, d) | (z == 0))
                def _():
                    passing(slot)

                @pl.when(whole(d))
                def _():
                    relay(1, 0, LEFT)
                    relay(3, 1, RIGHT)
            else:
                passing(slot)

        each(body, slots)

    def tail(t):
        @pl.when(whole(distance(t)) & (z <= reach[0]))
        def _():
            arrived(0, 0, LATE)
            for c, h in ((1, 1), (3, 0), (2, 0), (2, 1)):
                relay(c, h, LATE)

    def column(t):
        d = distance(t)

        def body(slot):
            for h in range(2):
                arrived(slot, z - d, COLUMN + h)
                along(slot, d, h)

        each(body)

    def settle(t):
        d = distance(t)
        w = z - d

        def body(slot):
            if slot == 0:
                @pl.when(plain(slot, d))
                def _():
                    arrived(slot, w, LATE)
            else:
                arrived(slot, w, LATE)
            store(slot, w).start()

        each(body)

    def finish(t):
        d = distance(t)
        w = z - d

        def body(slot):
            up, down = onward(slot, d)

            @pl.when(up | down)
            def _():
                sent(slot, up_sem.at[row(slot, w)], 2)

            @pl.when(plain(slot, d) | (z == 0))
            def _():
                sent(slot, beside_sem.at[row(slot, w)], 6)

            store(slot, w).wait()

        each(body)

    def column_copy(d):
        peer = (tp + d) % NTP
        first = pl.multiple_of(peer * SPAN, SPAN)
        return pltpu.make_async_remote_copy(
            src_ref=out_w.at[:, pl.ds(first, SPAN)], dst_ref=columns.at[tp],
            send_sem=once_sem.at[W_SEND], recv_sem=once_sem.at[W_RECV],
            device_id={"tp": peer}, device_id_type=MESH)

    def begin(slot):
        for h in range(2):
            along(slot, 0, h)

    @pl.when(low)
    def _():
        for h in range(2):
            to_top(h).start()

    each(begin, (0, 1))

    load_q.wait()
    for b in range(SEQS):
        q_out[b] = jnp.dot(rows_in[b], q_weights[...], preferred_element_type=jnp.float32).astype(jnp.bfloat16)
    make_plan(kv, lengths, chosen, plan, named, packed)

    around(0, (0,))
    each(begin, (2, 3))
    for d in range(1, NTP):
        column_copy(d).start()

    @pl.loop(1, NZ + 4)
    def _(t):
        @pl.when((t < NZ) & (distance(t) <= z))
        def _():
            column(t)

        @pl.when((t - 3 < NZ) & (t - 3 > 0) & (distance(jnp.maximum(t - 3, 0)) <= z))
        def _():
            around(t - 3)

        @pl.when(t == 1)
        def _():
            around(0, (1, 2, 3))

        @pl.when((t - 4 >= 0) & (t - 4 < NZ))
        def _():
            tail(jnp.maximum(t - 4, 0))

    @pl.loop(0, NZ)
    def _(t):
        @pl.when(distance(t) <= z)
        def _():
            settle(t)

    @pl.loop(0, NZ)
    def _(t):
        @pl.when(distance(t) <= z)
        def _():
            finish(t)

    @pl.when(low)
    def _():
        sent(0, once_sem.at[TO_TOP], 2)

    climbs = z <= reach[0]

    @pl.when(climbs & (z < 2))
    def _():
        sent(0, once_sem.at[RELAY_UP], 8)

    @pl.when(climbs & (z == 2))
    def _():
        sent(0, once_sem.at[RELAY_UP], 2)

    @pl.when(climbs & ((z == 0) | (z >= 6)))
    def _():
        sent(0, once_sem.at[RELAY_DOWN], 8)

    others = columns.at[pl.ds(0, NTP - 1)]
    pltpu.make_async_remote_copy(
        src_ref=others, dst_ref=others, send_sem=once_sem.at[W_SEND], recv_sem=once_sem.at[W_RECV],
        device_id=right, device_id_type=MESH).wait()


def spread(reach, lengths, chosen, inputs, query_weight, key_weight, value_weight, out_weight):
    dma = pltpu.SemaphoreType.DMA
    named = SEQS * (SPAN // KB)
    rows = sum(r + 1 for r in reach)
    return pl.pallas_call(
        lambda *refs: spread_kernel(reach, *refs),
        name="spread",
        out_shape=(
            jax.ShapeDtypeStruct((SEQS, NZ * NX * SPAN, 2 * HD), jnp.bfloat16),
            jax.ShapeDtypeStruct((NTP, SPAN, SPAN), jnp.bfloat16),
            jax.ShapeDtypeStruct((SEQS, SPAN, 2 * HD), jnp.bfloat16),
            jax.ShapeDtypeStruct((MORE + named, LANES), jnp.int32),
        ),
        in_specs=[SMEM, VMEM] + [ANY] * 5,
        out_specs=(ANY, ANY, VMEM, VMEM),
        scratch_shapes=[
            pltpu.VMEM((SEQS, NZ * NX * SPAN, 2 * HD), jnp.bfloat16),
            pltpu.VMEM((SEQS, SPAN, MODEL), jnp.bfloat16),
            pltpu.VMEM((MODEL, 2 * HD), jnp.bfloat16),
            pltpu.VMEM((MODEL, 2 * HD), jnp.bfloat16),
            pltpu.VMEM((SEQS, SPAN, 2 * HD), jnp.bfloat16),
            pltpu.VMEM((named, LANES), jnp.int32),
            pltpu.VMEM((MORE, LANES), jnp.int32),
            dma((SEQS + 3,)),
            dma((rows,)),
            dma((rows, 5)),
            dma((rows,)),
            dma((rows,)),
            dma((5,)),
        ],
        compiler_params=pltpu.CompilerParams(
            collective_id=0 if reach == REACH else 1, has_side_effects=True
        ),
    )(lengths, chosen, inputs, query_weight, key_weight, value_weight, out_weight)


def attend_kernel(lengths, plan, q, cache, out, keys, scores, high, total, acc, own_sems, sems):
    kv = lax.axis_index("kv")
    slots = plan[MORE, LIVE]
    blocks = SPAN // KB
    heads = 2

    def sequence(slot):
        b = plan[MORE, ORDER + slot]
        return b, plan[b, COUNT]

    def own_copy(slot):
        span = pl.ds(pl.multiple_of(kv * SPAN, SPAN), SPAN)
        return pltpu.make_async_copy(
            cache.at[slot, span], keys.at[slot % 2, pl.ds(0, SPAN)], own_sems.at[slot % 2])

    def block_copy(slot, block, e):
        row = pl.multiple_of(block * KB, KB)
        to = pl.multiple_of(SPAN + e * KB, KB)
        return pltpu.make_async_copy(
            cache.at[slot, pl.ds(row, KB)], keys.at[slot % 2, pl.ds(to, KB)], sems.at[slot % 2])

    def fetch(slot):
        b, n = sequence(slot)
        own_copy(slot).start()

        @pl.loop(0, n)
        def _(e):
            block_copy(slot, plan[b, e] % 256, e).start()

        past = pl.ds(pl.multiple_of(SPAN + n * KB, KB), 3 * KB)
        keys[slot % 2, past, :] = jnp.zeros((3 * KB, 2 * HD), jnp.bfloat16)

    def part(h, i):
        return slice(h * SPAN + i * KB, h * SPAN + (i + 1) * KB)

    def compute(slot):
        b, n = sequence(slot)
        held = keys.at[slot % 2]
        chunks = 1 + (n + 3) // 4
        own_copy(slot).wait()
        both = q[b]
        stacked = jnp.concatenate([both[:, :HD], both[:, HD:]], axis=0)
        lane = lax.broadcasted_iota(jnp.int32, (1, CHUNK), 1)
        place = lane // KB

        def score(first):
            return lax.dot_general(stacked, held[pl.ds(first, CHUNK), :HD], (((1,), (1,)), ((), ())),
                                   preferred_element_type=jnp.float32) * (HD ** -0.5)

        s = score(0)
        col = lax.broadcasted_iota(jnp.int32, (KB, CHUNK), 1)
        row = lax.broadcasted_iota(jnp.int32, (KB, CHUNK), 0)
        for i in range(blocks):
            bits = plan[MORE + b * 4 + i, LOCAL] | (1 << i)
            named = jnp.zeros((1, CHUNK), jnp.int32)
            for p in range(blocks):
                named = jnp.where(place == p, (bits >> p) & 1, named)
            limit = jnp.where(named != 0, lane, SPAN)
            for h in range(heads):
                now = jnp.where(limit <= row + i * KB, s[part(h, i)], -jnp.inf)
                scores[0, part(h, i), :] = now
                high[part(h, i), :] = jnp.maximum(now[:, :HD], now[:, HD:])

        @pl.loop(0, n)
        def _(e):
            block_copy(slot, 0, e).wait()

        @pl.loop(1, chunks)
        def _(c):
            s = score(pl.multiple_of(c * CHUNK, CHUNK))
            codes = []
            for p in range(blocks):
                e = (c - 1) * 4 + p
                codes.append(jnp.where(e < n, plan[b, e] // 256, 0))
            for i in range(blocks):
                shift = jnp.zeros((1, CHUNK), jnp.float32)
                for p in range(blocks):
                    absent = jnp.where((codes[p] >> i) & 1 != 0, jnp.float32(0), -jnp.inf)
                    shift = jnp.where(place == p, absent, shift)
                for h in range(heads):
                    now = s[part(h, i)] + shift
                    scores[c, part(h, i), :] = now
                    high[part(h, i), :] = jnp.maximum(high[part(h, i), :], jnp.maximum(now[:, :HD], now[:, HD:]))

        for h in range(heads):
            for i in range(blocks):
                top = jnp.max(high[part(h, i), :], axis=1, keepdims=True)
                high[part(h, i), :] = jnp.broadcast_to(top, (KB, HD))
        total[...] = jnp.zeros_like(total)

        @pl.loop(0, chunks)
        def _(c):
            for h in range(heads):
                for i in range(blocks):
                    top = high[part(h, i), :]
                    left = jnp.exp(scores[c, part(h, i), :HD] - top)
                    right = jnp.exp(scores[c, part(h, i), HD:] - top)
                    scores[c, part(h, i), :HD] = left
                    scores[c, part(h, i), HD:] = right
                    total[part(h, i), :] += left + right

        again = jnp.int32(0)
        for i in range(blocks):
            again += plan[MORE + b * 4 + i, REPEATS]

        def self_part(h, i):
            return jnp.where(col == row + i * KB, scores[0, part(h, i), :], 0.0)

        @pl.when(again > 0)
        def _():
            for h in range(heads):
                for i in range(blocks):
                    e = self_part(h, i)
                    times = plan[MORE + b * 4 + i, REPEATS].astype(jnp.float32)
                    total[part(h, i), :] += times * (e[:, :HD] + e[:, HD:])

        for h in range(heads):
            for i in range(blocks):
                share = 1.0 / jnp.sum(total[part(h, i), :], axis=1, keepdims=True)
                total[part(h, i), :] = jnp.broadcast_to(share, (KB, HD))
        acc[...] = jnp.zeros_like(acc)

        @pl.when(again > 0)
        def _():
            for h in range(heads):
                for i in range(blocks):
                    share = total[part(h, i), :]
                    e = self_part(h, i)
                    weight = jnp.concatenate([e[:, :HD] * share, e[:, HD:] * share], axis=1)
                    times = plan[MORE + b * 4 + i, REPEATS].astype(jnp.float32)
                    acc[part(h, i), :] = times * jnp.dot(
                        weight.astype(jnp.bfloat16), held[:SPAN, HD:], preferred_element_type=jnp.float32)

        @pl.loop(0, chunks)
        def _(c):
            share = total[...]
            weight = jnp.concatenate([scores[c, :, :HD] * share, scores[c, :, HD:] * share], axis=1)
            acc[...] += jnp.dot(weight.astype(jnp.bfloat16),
                                held[pl.ds(pl.multiple_of(c * CHUNK, CHUNK), CHUNK), HD:],
                                preferred_element_type=jnp.float32)

        pos = kv * SPAN + lax.broadcasted_iota(jnp.int32, (SPAN, HD), 0)
        for h in range(heads):
            done = jnp.where(pos < lengths[b], acc[h * SPAN:(h + 1) * SPAN, :], 0.0)
            out[slot, :, h * HD:(h + 1) * HD] = done.astype(jnp.bfloat16)

    @pl.loop(slots, SEQS)
    def _(slot):
        out[slot] = jnp.zeros((SPAN, 2 * HD), jnp.bfloat16)

    @pl.when(slots > 0)
    def _():
        fetch(jnp.int32(0))

    @pl.loop(0, slots)
    def _(slot):
        @pl.when(slot + 1 < slots)
        def _():
            fetch(slot + 1)

        compute(slot)


def attend(lengths, plan, q, cache):
    most = NZ * NX * (SPAN // KB)
    rows = 2 * SPAN
    return pl.pallas_call(
        attend_kernel,
        name="attend",
        out_shape=jax.ShapeDtypeStruct((SEQS, SPAN, 2 * HD), jnp.bfloat16),
        in_specs=[SMEM, SMEM, VMEM, ANY],
        out_specs=VMEM,
        scratch_shapes=[
            pltpu.VMEM((2, SPAN + most * KB, 2 * HD), jnp.bfloat16),
            pltpu.VMEM((1 + most // 4, rows, CHUNK), jnp.float32),
            pltpu.VMEM((rows, HD), jnp.float32),
            pltpu.VMEM((rows, HD), jnp.float32),
            pltpu.VMEM((rows, HD), jnp.float32),
            pltpu.SemaphoreType.DMA((2,)),
            pltpu.SemaphoreType.DMA((2,)),
        ],
    )(lengths, plan, q, cache)


def mix_kernel(reach, lengths, own, columns, out_w, out, groups, own_w, acc, load_sem, next_recv,
               prev_recv, core_recv, sent):
    kv, tp = lax.axis_index("kv"), lax.axis_index("tp")
    z = kv // NX
    y, core = tp // 2, tp % 2
    y_next, y_prev, y_far = (y + 1) % NY, (y + NY - 1) % NY, (y + 2) % NY
    after, before = {"tp": y_next * 2 + core}, {"tp": y_prev * 2 + core}
    partner = {"tp": y * 2 + 1 - core}
    half = SPAN // 2

    load = pltpu.make_async_copy(out_w.at[:, pl.ds(pl.multiple_of(tp * SPAN, SPAN), SPAN)], own_w, load_sem)
    load.start()
    barrier = pltpu.get_barrier_semaphore()
    for d in (after, before, partner):
        pl.semaphore_signal(barrier, inc=1, device_id=d, device_id_type=MESH)
    load.wait()
    pl.semaphore_wait(barrier, 3)

    def piece(owner_y, owner_core, slot, h):
        return groups.at[owner_y * 2 + owner_core, slot, pl.ds(h * half, half)]

    def copy(src, dst, send_sem, recv_sem, device):
        return pltpu.make_async_remote_copy(
            src_ref=src, dst_ref=dst, send_sem=send_sem, recv_sem=recv_sem,
            device_id=device, device_id_type=MESH)

    def mine(slot, h):
        return own.at[slot, pl.ds(h * half, half)]

    def to_next(slot, h):
        return copy(mine(slot, h), piece(y, core, slot, h), sent.at[slot], next_recv.at[h, slot], after)

    def to_prev(slot, h):
        return copy(mine(slot, h), piece(y, core, slot, h), sent.at[slot], prev_recv.at[h, slot], before)

    def on_next(slot):
        here = piece(y_prev, core, slot, 0)
        return copy(here, here, sent.at[slot], next_recv.at[2, slot], after)

    def on_prev(slot):
        here = piece(y_next, core, slot, 1)
        return copy(here, here, sent.at[slot], prev_recv.at[2, slot], before)

    def across(stage, owner_y, slot, h, src=None):
        here = piece(owner_y, core, slot, h)
        return copy(here if src is None else src, here, sent.at[slot], core_recv.at[stage, slot], partner)

    def crossed(stage, slot):
        both = groups.at[0, slot]
        copy(both, both, sent.at[slot], core_recv.at[stage, slot], partner).wait_recv()

    def each(body):
        for slot in range(SEQS):
            @pl.when(z <= reach[slot])
            def _(slot=slot):
                body(slot)

    def product(rows, weight):
        part = jnp.dot(rows, weight, preferred_element_type=jnp.float32)
        return part.astype(jnp.bfloat16).astype(jnp.float32)

    def add(slot, owner_y, owner_core):
        g = owner_y * 2 + owner_core
        acc[slot] += product(groups[g, slot], columns[g])

    def begin(slot):
        to_next(slot, 0).start()
        to_prev(slot, 1).start()
        to_next(slot, 1).start()
        to_prev(slot, 0).start()
        for h in range(2):
            across(0, y, slot, h, mine(slot, h)).start()

    def first(slot):
        acc[slot] = product(own[slot], own_w[...])

    def relay(slot):
        to_next(slot, 0).wait_recv()
        on_next(slot).start()
        across(1, y_prev, slot, 0).start()
        to_prev(slot, 1).wait_recv()
        on_prev(slot).start()
        across(2, y_next, slot, 1).start()
        to_next(slot, 1).wait_recv()
        across(1, y_prev, slot, 1).start()
        to_prev(slot, 0).wait_recv()
        across(2, y_next, slot, 0).start()

    def near(slot):
        crossed(0, slot)
        for owner_y, owner_core in ((y, 1 - core), (y_prev, core), (y_next, core)):
            add(slot, owner_y, owner_core)

    def far(slot):
        on_next(slot).wait_recv()
        across(3, y_far, slot, 0).start()
        on_prev(slot).wait_recv()
        across(3, y_far, slot, 1).start()
        for stage, owner_y in ((1, y_prev), (2, y_next)):
            crossed(stage, slot)
            add(slot, owner_y, 1 - core)
        add(slot, y_far, core)

    def last(slot):
        crossed(3, slot)
        add(slot, y_far, 1 - core)

    def finish(slot):
        all_sent = groups.at[pl.ds(0, 7), slot]
        copy(all_sent, all_sent, sent.at[slot], core_recv.at[0, slot], partner).wait_send()

    each(begin)
    acc[...] = jnp.zeros_like(acc)
    each(first)

    def both(slot):
        relay(slot)
        near(slot)

    each(both)
    each(far)
    each(last)
    for b in range(SEQS):
        slot = jnp.int32(0)
        for o in range(SEQS):
            if o < b:
                slot += (lengths[o] >= lengths[b]).astype(jnp.int32)
            elif o > b:
                slot += (lengths[o] > lengths[b]).astype(jnp.int32)
        out[b] = acc[slot].astype(jnp.bfloat16)
    each(finish)


def mix(reach, lengths, own, columns, out_weight):
    dma = pltpu.SemaphoreType.DMA
    return pl.pallas_call(
        lambda *refs: mix_kernel(reach, *refs),
        name="mix",
        out_shape=jax.ShapeDtypeStruct((SEQS, SPAN, SPAN), jnp.bfloat16),
        in_specs=[SMEM, VMEM, VMEM, ANY],
        out_specs=VMEM,
        scratch_shapes=[
            pltpu.VMEM((NTP, SEQS, SPAN, 2 * HD), jnp.bfloat16),
            pltpu.VMEM((SPAN, SPAN), jnp.bfloat16),
            pltpu.VMEM((SEQS, SPAN, SPAN), jnp.float32),
            dma,
            dma((3, SEQS)),
            dma((3, SEQS)),
            dma((4, SEQS)),
            dma((SEQS,)),
        ],
        compiler_params=pltpu.CompilerParams(
            collective_id=2 if reach == REACH else 3, has_side_effects=True
        ),
    )(lengths, own, columns, out_weight)


def shards(inputs, query_weight, key_weight, value_weight, out_weight, chosen, lengths):
    def rest(reach):
        cache, columns, queries, plan = spread(
            reach, lengths, chosen, inputs, query_weight, key_weight, value_weight, out_weight)
        attended = attend(lengths, plan, queries, cache)
        return mix(reach, lengths, attended, columns, out_weight)

    score = jnp.where(lengths > 3072, 6, jnp.where(lengths > 2048, 3, jnp.where(lengths > 1024, 2, 0)))
    near = jnp.sum(score) < 12
    return lax.cond(near, lambda: rest(NEAR_REACH), lambda: rest(REACH))


def solution(mesh):
    placed = (
        P(None, "kv", None),
        P(None, "tp"),
        P(None, "tp"),
        P(None, "tp"),
        P("tp", None),
        P(None, "kv", None),
        P(),
    )
    return jax.shard_map(
        shards, mesh=mesh, in_specs=placed, out_specs=P(None, "kv", "tp"), check_vma=False
    )
```

time: 81.8 us -> 66.1 us (0.81)
  Pallas kernels: 76.8 us -> 62.9 us
  between operations: 1.95 us -> 0.66 us
    pallas_call x3 -> x1, Pallas kernels: 37.4 us -> 25.9 us  [mix(): pl.pallas_call(lambda *refs: mix_kernel(reach, *refs), name='mix', out_sh...]
    pallas_call x1, Pallas kernels: 31.9 us -> 29.6 us  [spread(): pl.pallas_call(lambda *refs: spread_kernel(reach, *refs), name='spread',...]
where the time goes in v1:
time: 66.1 us; the launch traced here: 65.9 us
  Pallas kernels  62.9 us (95%)
  other arithmetic  1.29 us (2%)
  local copies, waits for them, and re-layouts  0.81 us (1%)
    pallas_call x1, Pallas kernels, spread(): pl.pallas_call(lambda *refs: spread_kernel(reach, *refs), name='spread',...  29.6 us
    pallas_call x1, Pallas kernels, mix(): pl.pallas_call(lambda *refs: mix_kernel(reach, *refs), name='mix', out_sh...  25.9 us
    pallas_call x1, Pallas kernels, attend(): pl.pallas_call(attend_kernel, name='attend', out_shape=jax.ShapeDtypeStru...  7.45 us

profile of v1, /device:TPU:1, one launch (start us, length us, event | category | flops | bytes accessed | tf_op | source)
XLA Modules:
  0.0 65.9 jit_solution(13052680328486239216)
XLA Ops:
  0.0 1.3 %fusion = s32[]{:T(128)} fusion(s32[4]{0:T(128)} %param.15), kind=kLoop, calls=%fused_computation.3 | loop fusion | flops 27 | bytes 20 | tf_op jit(solution)/shard_map/reduce_sum | solution.py:793
  1.9 63.2 %conditional.1 = (bf16[4,256,256]{2,1,0:T(8,128)(2,1)S(1)}) conditional(s32[]{:T(128)} %convert_element_type.3, (s32[4]{0:T(128)}, s32[4,4,32]{2,1,0:T(4,128)}, bf16[4,256,2048]{2,1,0:T(8,128)(2,1)}, bf16[2048,256]{1,0:T(8,128)(2,1)}, bf16[2048,128]{1,0:T(8,128)(2,1)}, /*index=5*/bf16[2048,128]{1,0:T(8,128)(2,1)}, ...), branch_computations={%region_1.2_spmd, %region_2.3_spmd} | conditional | bytes 4194432 | solution.py:794
  2.0 0.0 copy-start.1
  2.0 0.0 copy-start.3
  2.0 29.6 %spread.3 = (bf16[4,8192,256]{2,1,0:T(8,128)(2,1)}, bf16[8,256,256]{2,1,0:T(8,128)(2,1)}, bf16[4,256,256]{2,1,0:T(8,128)(2,1)}, s32[24,128]{1,0:T(8,128)}) custom-call(s32[4]{0:T(128)} %get-tuple-element.47.refs_0_.lengths, s32[4,4,32]{2,1,0:T(4,128)} %get-tuple-element.48.refs_1_, bf16[4,256,2048]{2,1,0:T(8,128)(2,1)} %get-tuple-element.49.refs_2_, ...), custom_call_target="tpu_custom_call" | custom-call | tf_op jit(solution)/shard_map/cond/branch_1_fun/spread/pallas_call | solution.py:412
  31.5 7.5 %attend.3.refs_1_ = bf16[4,256,256]{2,1,0:T(8,128)(2,1)} custom-call(s32[4]{0:T(128)} %get-tuple-element.47.refs_0_.lengths, s32[24,128]{1,0:T(8,128)} %get-tuple-element.54.plan, bf16[4,256,256]{2,1,0:T(8,128)(2,1)} %get-tuple-element.55.q, bf16[4,8192,256]{2,1,0:T(8,128)(2,1)} %get-tuple-element.56.cache), custom_call_target="tpu_custom_call" | custom-call | tf_op jit(solution)/shard_map/cond/branch_1_fun/attend/pallas_call | solution.py:610
  39.0 0.0 copy-done.1
  39.0 0.0 copy-done.3
  39.0 25.9 %mix.3 = bf16[4,256,256]{2,1,0:T(8,128)(2,1)S(1)} custom-call(s32[4]{0:T(128)S(1)} %copy-done.3, bf16[4,256,256]{2,1,0:T(8,128)(2,1)} %attend.3.refs_1_, bf16[8,256,256]{2,1,0:T(8,128)(2,1)} %get-tuple-element.57.refs_2_, bf16[256,2048]{1,0:T(8,128)(2,1)S(1)} %copy-done.1), custom_call_target="tpu_custom_call" | custom-call | tf_op jit(solution)/shard_map/cond/branch_1_fun/mix/pallas_call | solution.py:763
  65.1 0.8 %copy.13 = bf16[4,256,256]{2,1,0:T(8,128)(2,1)} copy(bf16[4,256,256]{2,1,0:T(8,128)(2,1)S(1)} %get-tuple-element.58) | data formatting | bytes 1048576
Async XLA Ops:
  2.0 37.0 %copy-start.1 = (bf16[256,2048]{1,0:T(8,128)(2,1)S(1)}, bf16[256,2048]{1,0:T(8,128)(2,1)}, u32[]{:S(2)}) copy-start(bf16[256,2048]{1,0:T(8,128)(2,1)} %get-tuple-element.53.refs_6_.refs_3_) | copy-start | bytes 3145732 | tf_op jit(solution)/shard_map/cond
  2.0 37.0 %copy-start.3 = (s32[4]{0:T(128)S(1)}, s32[4]{0:T(128)}, u32[]{:S(2)}) copy-start(s32[4]{0:T(128)} %get-tuple-element.47.refs_0_.lengths) | copy-start | bytes 52 | tf_op jit(solution)/shard_map/cond
